TPU v7x, 512 devices: a whole 4x4x16 slice. The times are simulated.
512 devices in a mesh: ep: 32 (over z, core), tp: 16 (over y, x).
Axes of the slice: x: 4, y: 4, z: 16, core: 2. Of those that a mesh axis runs over, the one named last changes fastest.
Arguments:
- tokens: bfloat16 [4096, 2048], P('ep'), may hold values from -6 to 6
- routes: int32 [4096, 2], P('ep'), may hold values from 0 to 15, all different within a row; in each aligned block of 128 rows (0 to 127, 128 to 255, ...) at most 18 rows name the same one
- route_weights: float32 [4096, 2], P('ep'), may hold values from 0.2 to 1
- out_grad: bfloat16 [4096, 2048], P('ep'), may hold values from -6 to 6
- gate_proj: bfloat16 [32, 2048, 2048], P('ep', None, 'tp'), may hold values from -0.125 to 0.125
- up_proj: bfloat16 [32, 2048, 2048], P('ep', None, 'tp'), may hold values from -0.125 to 0.125
- down_proj: bfloat16 [32, 2048, 2048], P('ep', 'tp'), may hold values from -0.09375 to 0.09375
Outputs:
- tokens_grad: bfloat16 [4096, 2048], P('ep', 'tp')
- route_grad: float32 [4096, 2], P('ep')
- gate_grad: bfloat16 [32, 2048, 2048], P('ep', None, 'tp')
- up_grad: bfloat16 [32, 2048, 2048], P('ep', None, 'tp')
- down_grad: bfloat16 [32, 2048, 2048], P('ep', 'tp')
Inputs may be any that keep to these rules, and one draw needn't show every extreme that they name: `routes`: each row names 2 different experts. In the rows of one device (an aligned block of 128 rows) no expert is named more than 18 times, and in some blocks one expert is named exactly 18 times.
All inputs are finite; a program needn't handle non-finite values.
Results may differ from a plain program's by a relative error of at most 0.019.
Values may be sent and summed in bfloat16 or wider, within the bound.
No kernel may reach another device: no remote copies, remote signals or barrier semaphores. Data moves between devices by JAX's collectives and lax.ppermute only.
A program may use at most 64 MiB of HBM per device.

v0:
```python
import jax
import jax.numpy as jnp
from jax import lax
from jax.experimental import pallas as pl
from jax.experimental.pallas import tpu as pltpu
from jax.sharding import Mesh
from jax.sharding import PartitionSpec as P


EP = ("ep_0", "ep_1")
BF = jnp.bfloat16
F32 = jnp.float32

CAP = 18
SRC = 16
ROWS = SRC * CAP
PIECE = 36
BACK = 20
GATH = 2 * ROWS
PART = ROWS + 8
TP_ORDER = (10, 11, 15, 14, 13, 12, 0, 1, 2, 3, 7, 6, 5, 4, 8, 9)
TP_PLACE = tuple(TP_ORDER.index(t) for t in range(16))
LIMIT = pltpu.CompilerParams(vmem_limit_bytes=24 * 1024 * 1024)


def iota(shape, dim):
    return lax.broadcasted_iota(jnp.int32, shape, dim)


def one_if(cond):
    return jnp.where(cond, 1.0, 0.0).astype(BF)


def split_two(value):
    high = value.astype(BF)
    low = (value - high.astype(F32)).astype(BF)
    return high, low


def contract_cols(left, right):
    return lax.dot_general(left, right, (((1,), (1,)), ((), ())), preferred_element_type=F32)


def matmul(left, right):
    return lax.dot_general(left, right, (((1,), (0,)), ((), ())), preferred_element_type=F32)


def member_at(place):
    return (place + 8) & 15


def own_lanes():
    z = lax.axis_index("ep_0")
    place = (z + 8) % 16
    return (place % 4) * 32


def expand(expert, values):
    return matmul(one_if(iota((expert.shape[0], 16), 1) == expert), values)


def ranks(routes):
    count = routes.shape[1]
    expert = iota((16, count), 0)
    first = routes[0:1, :] == expert
    second = routes[1:2, :] == expert
    member = jnp.where(first | second, 1.0, 0.0)
    before = one_if(iota((count, count), 0) < iota((count, count), 1))
    rank = matmul(member.astype(BF), before)
    return first, second, member, rank


def dispatch_kernel(
    routes_hbm,
    weights_hbm,
    tokens_ref,
    grad_ref,
    gate,
    up,
    down,
    out_ref,
    swap_ref,
    data_ref,
    routes_ref,
    weights_ref,
    sems,
    move_sems,
):
    start = pl.multiple_of(lax.axis_index("tp") * 128, 128)
    small = [
        pltpu.make_async_copy(routes_hbm, routes_ref, sems.at[2]),
        pltpu.make_async_copy(weights_hbm, weights_ref, sems.at[3]),
    ]
    loads = [
        pltpu.make_async_copy(
            ref.at[:, pl.ds(start, 128)], data_ref.at[pl.ds(128 * k, 128), :], sems.at[k]
        )
        for k, ref in enumerate((tokens_ref, grad_ref))
    ]
    for load in small + loads:
        load.start()
    moves = [
        pltpu.make_async_copy(ref, swap_ref.at[pl.ds(2048 * k, 2048), :], move_sems.at[16 + k])
        for k, ref in enumerate((gate, up))
    ] + [
        pltpu.make_async_copy(
            down.at[:, pl.ds(128 * t, 128)], swap_ref.at[pl.ds(4096 + 128 * t, 128), :], move_sems.at[t]
        )
        for t in range(16)
    ]
    for move in moves:
        move.start()
    for load in small:
        load.wait()
    first, second, member, rank = ranks(routes_ref[...])
    weights = weights_ref[...]
    weight = jnp.where(first, weights[0:1, :], 0.0) + jnp.where(second, weights[1:2, :], 0.0)
    slot = jnp.where(member > 0.0, rank, -100.0)
    row = iota((16 * PIECE, 1), 0)
    place = (row * 1821) >> 16
    expert = member_at(place)
    slots = expand(expert, slot.astype(BF)).astype(jnp.int32)
    within = row - place * PIECE
    sel_x = slots == within
    sel_dy = slots + CAP == within
    high, low = split_two(weight)
    spread = expand(expert, high) + expand(expert, low)
    factor = jnp.sum(jnp.where(sel_dy, spread, 0.0), axis=1, keepdims=True)
    factor = jnp.where(within < CAP, 1.0, factor)
    chosen = jnp.concatenate([one_if(sel_x), one_if(sel_dy)], axis=1)
    for load in loads:
        load.wait()
    out_ref[...] = (matmul(chosen, data_ref[...]) * factor).astype(BF)
    for move in moves:
        move.wait()


def plan_kernel(copies_ref):
    p = iota((GATH, 1), 0)
    is_dy = p >= ROWS
    q = jnp.where(is_dy, p - ROWS, p)
    source = (q * 3641) >> 16
    target = source * PIECE + (q - source * CAP) + jnp.where(is_dy, CAP, 0)
    copies_ref[...] = one_if(iota((GATH, SRC * PIECE), 1) == target)


def places_kernel(routes_hbm, weights_hbm, combine_ref, lanes_ref, routes_ref, weights_ref, sems):
    loads = [
        pltpu.make_async_copy(routes_hbm, routes_ref, sems.at[0]),
        pltpu.make_async_copy(weights_hbm, weights_ref, sems.at[1]),
    ]
    for load in loads:
        load.start()
    for load in loads:
        load.wait()
    routes = routes_ref[...]
    first, second, member, rank = ranks(routes)
    slot = jnp.where(member > 0.0, rank, -100.0)
    row = iota((16 * BACK, 1), 0)
    place = (row * 3277) >> 16
    expert = member_at(place)
    within = row - place * BACK
    sel = jnp.where(expand(expert, slot.astype(BF)).astype(jnp.int32) == within, 1.0, 0.0)
    combine_ref[0:128, :] = jnp.transpose(sel).astype(BF)
    offset = own_lanes()
    weights = weights_ref[...]
    for k, mine in enumerate((first, second)):
        sel = jnp.where(within >= CAP, expand(expert, one_if(mine)), 0.0)
        combine_ref[128 * (k + 1) : 128 * (k + 2), :] = jnp.transpose(sel).astype(BF)
        index = jnp.sum(jnp.where(mine, rank, 0.0), axis=0, keepdims=True).astype(jnp.int32)
        lanes = jnp.where(iota((128, 128), 0) == index + offset, 1.0 / weights[k : k + 1, :], 0.0)
        lanes_ref[128 * k : 128 * (k + 1), :] = jnp.transpose(lanes)


def settle_kernel(in_ref, out_ref):
    del in_ref, out_ref


def copies_kernel(in_ref, pick_ref, out_ref):
    rows = matmul(pick_ref[...], in_ref[...]).astype(BF)
    for t in range(16):
        out_ref[t] = rows


def lane_of_row():
    r = iota((ROWS, 1), 0)
    source = (r * 3641) >> 16
    lane = (source & 3) * 32 + (r - source * CAP)
    return source >> 2, lane


def pair_cols(ref, t, start):
    return jnp.concatenate([ref[TP_PLACE[2 * t + k], start : start + ROWS, :] for k in range(2)], axis=1)


def main_kernel(own_ref, gate, up, down, swap_ref, part_out, both_ref, hidden_ref, part_ref, sems):
    pre_gate = jnp.zeros((ROWS, 256), F32)
    pre_up = jnp.zeros((ROWS, 256), F32)
    d_hidden = jnp.zeros((ROWS, 256), F32)

    def both_halves(ref, t, first):
        cols = slice(256 * t, 256 * t + 256)
        return jnp.concatenate([ref[cols, :], swap_ref[first + 256 * t : first + 256 * t + 256, :]], axis=1)

    for t in range(8):
        x = pair_cols(own_ref, t, 0)
        pre_gate = pre_gate + matmul(x, both_halves(gate, t, 0))
        pre_up = pre_up + matmul(x, both_halves(up, t, 2048))
        at = 4096 + 256 * t
        down_2 = jnp.concatenate([swap_ref[at : at + 128, :], swap_ref[at + 128 : at + 256, :]], axis=1)
        d_hidden = d_hidden + contract_cols(
            pair_cols(own_ref, t, ROWS),
            jnp.concatenate([down[:, 256 * t : 256 * t + 256], down_2], axis=0),
        )
    sigma = jax.nn.sigmoid(pre_gate)
    activ = pre_gate * sigma
    hidden = activ * pre_up
    gate_part = jnp.sum(hidden * d_hidden, axis=1, keepdims=True)
    d_gate = (d_hidden * pre_up * sigma * (1.0 + pre_gate * (1.0 - sigma))).astype(BF)
    d_up = (d_hidden * activ).astype(BF)
    both_ref[:, 0:256] = d_gate
    both_ref[:, 256:512] = d_up
    hidden_ref[...] = hidden.astype(BF)
    _, lane = lane_of_row()
    spread = jnp.where(iota((ROWS, 128), 1) == lane, gate_part, 0.0)
    packed = jnp.sum(spread.reshape(4, ROWS // 4, 128), axis=1)
    extra = jnp.concatenate(split_two(packed), axis=0)
    stores = []
    for t in range(8):
        value = contract_cols(d_gate, both_halves(gate, t, 0))
        value = value + contract_cols(d_up, both_halves(up, t, 2048))
        value = value.astype(BF)
        for k in range(2):
            place = TP_PLACE[2 * t + k]
            part_ref[place, 0:ROWS, :] = value[:, 128 * k : 128 * k + 128]
            part_ref[place, ROWS:PART, :] = extra
            stores.append(pltpu.make_async_copy(part_ref.at[place], part_out.at[place], sems.at[place]))
            stores[-1].start()
    for store in stores:
        store.wait()


def half_grads(own_ref, both_ref, hidden_ref, half):
    lanes = slice(128 * half, 128 * half + 128)
    late = slice(256 + 128 * half, 256 + 128 * half + 128)
    both = jnp.concatenate([both_ref[:, lanes], both_ref[:, late]], axis=1)
    both_t = jnp.transpose(both.astype(F32)).astype(BF)
    hidden_t = jnp.transpose(hidden_ref[:, lanes].astype(F32)).astype(BF)
    for t in range(8):
        cols = slice(256 * t, 256 * t + 256)
        grads = matmul(both_t, pair_cols(own_ref, t, 0))
        yield cols, grads, matmul(hidden_t, pair_cols(own_ref, t, ROWS))


def partner_grads_kernel(own_ref, both_ref, hidden_ref, out_ref):
    for cols, both, down in half_grads(own_ref, both_ref, hidden_ref, 1):
        out_ref[0:256, cols] = both.astype(BF)
        out_ref[256:384, cols] = down.astype(BF)


def own_grads_kernel(own_ref, both_ref, hidden_ref, other_ref, gate_out, up_out, down_out):
    for cols, both, down in half_grads(own_ref, both_ref, hidden_ref, 0):
        grads = jnp.transpose(both + other_ref[0:256, cols].astype(F32))
        gate_out[cols, :] = grads[:, :128].astype(BF)
        up_out[cols, :] = grads[:, 128:].astype(BF)
        down_out[:, cols] = (down + other_ref[256:384, cols].astype(F32)).astype(BF)


def sum_kernel(in_ref, out_ref):
    rows = in_ref[0].astype(F32)
    for t in range(1, 16):
        rows = rows + in_ref[t].astype(F32)
    packed = rows[ROWS : ROWS + 4] + rows[ROWS + 4 : PART]
    high = packed.astype(BF).astype(F32)
    rows = jnp.concatenate([rows[:ROWS], high, packed - high], axis=0).astype(BF)
    p = iota((SRC * BACK, 1), 0)
    source = (p * 3277) >> 16
    j = p - source * BACK
    target = jnp.where(j < CAP, source * CAP + j, -1)
    target = jnp.where(j == 18, ROWS + (source >> 2), target)
    target = jnp.where(j == 19, ROWS + 4 + (source >> 2), target)
    pick = one_if(iota((SRC * BACK, PART), 1) == target)
    out_ref[...] = matmul(pick, rows).astype(BF)


def combine_kernel(in_ref, pick_ref, lanes_ref, tokens_ref, route_ref):
    values = matmul(pick_ref[...], in_ref[...])
    tokens_ref[...] = values[:128].astype(BF)
    gates = lax.dot_general(
        jnp.ones((8, 128), F32),
        values[128:] * lanes_ref[...],
        (((1,), (1,)), ((), ())),
        precision=lax.Precision.HIGHEST,
        preferred_element_type=F32,
    )
    route_ref[0:1, :] = gates[0:1, :128]
    route_ref[1:2, :] = gates[0:1, 128:]


def shape(dims, dtype=BF):
    return jax.ShapeDtypeStruct(dims, dtype)


def far_shape(dims, dtype=BF):
    return pltpu.HBM(dims, dtype)


def near(dims, dtype=BF):
    return pltpu.VMEM(dims, dtype)


def far(value):
    return pltpu.with_memory_space_constraint(value, pltpu.HBM)


def hold(value):
    return pltpu.with_memory_space_constraint(value, pltpu.VMEM)


def local(tokens, routes, route_weights, out_grad, gate_proj, up_proj, down_proj):
    return steps(tokens, routes, route_weights, out_grad, gate_proj[0], up_proj[0], down_proj[0])


def exchange(value, axis):
    groups = [[(k + 8) % 16 for k in range(16)]] if axis == "ep_0" else [list(TP_ORDER)]
    return lax.all_to_all(value, axis, 0, 0, axis_index_groups=groups, tiled=True)


def to_partner(value):
    return lax.ppermute(value, "ep_1", [(0, 1), (1, 0)])


def kernel(body, **settings):
    return pl.pallas_call(body, compiler_params=LIMIT, **settings)


def steps(tokens, routes, route_weights, out_grad, gate, up, down):
    count, width = tokens.shape
    routes_t = routes.T
    weights_t = route_weights.T
    vmem = pl.BlockSpec(memory_space=pltpu.VMEM)
    hbm = pl.BlockSpec(memory_space=pltpu.HBM)
    small = [pltpu.VMEM((2, count), jnp.int32), pltpu.VMEM((2, count), F32)]
    pieces, packed = kernel(
        dispatch_kernel,
        in_specs=[hbm] * 7,
        out_specs=(vmem, vmem),
        out_shape=(near((16 * PIECE, 128)), near((3 * width, 128))),
        scratch_shapes=[
            pltpu.VMEM((256, 128), BF),
            *small,
            pltpu.SemaphoreType.DMA((4,)),
            pltpu.SemaphoreType.DMA((18,)),
        ],
    )(far(routes_t), far(weights_t), far(tokens), far(out_grad), far(gate), far(up), far(down))
    received = exchange(pieces.reshape(16, PIECE // 4, 4, 128), "ep_0")
    pick_copies = kernel(plan_kernel, out_specs=vmem, out_shape=near((GATH, SRC * PIECE)))()
    packed_2 = to_partner(packed)
    packed_2 = kernel(
        settle_kernel,
        in_specs=[hbm],
        out_specs=hbm,
        out_shape=far_shape((3 * width, 128)),
        input_output_aliases={0: 0},
    )(far(packed_2))
    copies = kernel(copies_kernel, out_shape=near((16, GATH, 128)))(
        hold(received.reshape(SRC * PIECE, 128)), hold(pick_copies)
    )
    gathered = exchange(copies, "tp")
    own, own_far = hold(gathered), far(gathered)
    part, both, hidden = kernel(
        main_kernel,
        in_specs=[vmem] * 5,
        out_specs=(hbm, vmem, vmem),
        out_shape=(far_shape((16, PART, 128)), near((ROWS, 512)), near((ROWS, 256))),
        scratch_shapes=[pltpu.VMEM((16, PART, 128), BF), pltpu.SemaphoreType.DMA((16,))],
    )(own, gate, up, down, packed_2)
    spread = exchange(part, "tp")
    partner = kernel(partner_grads_kernel, out_shape=shape((384, width)))(own_far, both, hidden)
    mine = to_partner(partner)
    gate_grad, up_grad, down_grad = kernel(
        own_grads_kernel, out_shape=(shape((width, 128)), shape((width, 128)), shape((128, width)))
    )(own_far, both, hidden, mine)
    back = kernel(sum_kernel, out_shape=near((SRC * BACK, 128)))(hold(spread))
    pick_combine, lanes = kernel(
        places_kernel,
        in_specs=[hbm] * 2,
        out_specs=(vmem, vmem),
        out_shape=(near((384, 16 * BACK)), near((256, 128), F32)),
        scratch_shapes=[*small, pltpu.SemaphoreType.DMA((2,))],
    )(far(routes_t), far(weights_t))
    home = exchange(back.reshape(SRC, BACK // 4, 4, 128), "ep_0")
    tokens_grad, route_grad = kernel(
        combine_kernel, out_shape=(shape((count, 128)), shape((2, count), F32))
    )(hold(home.reshape(16 * BACK, 128)), hold(pick_combine), hold(lanes))
    return (tokens_grad, route_grad.T, gate_grad[None], up_grad[None], down_grad[None])


def solution(mesh):
    torus = Mesh(mesh.devices.reshape(16, 2, mesh.shape["tp"]), ("ep_0", "ep_1", "tp"))
    placed = (
        P(EP, None),
        P(EP, None),
        P(EP, None),
        P(EP, None),
        P(EP, None, "tp"),
        P(EP, None, "tp"),
        P(EP, "tp", None),
    )
    return jax.shard_map(
        local,
        mesh=torus,
        in_specs=placed,
        out_specs=(
            P(EP, "tp"),
            P(EP, None),
            P(EP, None, "tp"),
            P(EP, None, "tp"),
            P(EP, "tp", None),
        ),
        check_vma=False,
    )
```

profile of v0, /device:TPU:1, one launch (start us, length us, event | category | flops | bytes accessed | tf_op | source)
XLA Modules:
  0.0 130.7 jit_solution(7575733874034347968)
XLA Ops:
  0.6 2.9 %shard_map.110 = (bf16[576,128]{1,0:T(8,128)(2,1)}, bf16[6144,128]{1,0:T(8,128)(2,1)S(1)}) custom-call(s32[2,128]{1,0:T(2,128)} %bitcast.21, f32[2,128]{1,0:T(2,128)} %bitcast.23, bf16[128,2048]{1,0:T(8,128)(2,1)} %tokens_ref.1, bf16[128,2048]{1,0:T(8,128)(2,1)} %grad_ref.1, bf16[2048,128]{1,0:T(8,128)(2,1)} %bitcast.13, bf16[2048,128]{1,0:T(8,128)(2,1)} %bitcast.15, ...), custom_call_target="tpu_custom_call" | custom-call | tf_op jit(solution)/shard_map/pallas_call | solution.py:344
  3.5 0.0 copy-start.15
  3.5 1.1 copy-done.15
  4.7 19.1 %all-to-all-start = ((bf16[16,9,4,128]{3,2,1,0:T(4,128)(2,1)}), bf16[16,9,4,128]{3,2,1,0:T(4,128)(2,1)S(1)}, u32[]{:S(2)}, u32[]{:S(2)}) async-start(bf16[16,9,4,128]{3,2,1,0:T(4,128)(2,1)} %bitcast.5), calls=%async_computation | async-start | bytes 294912 | tf_op jit(solution)/shard_map/all_to_all | solution.py:326
  23.8 0.2 shard_map.111.pick_ref
  24.0 7.1 %all-to-all-done = bf16[16,9,4,128]{3,2,1,0:T(4,128)(2,1)S(1)} async-done(((bf16[16,9,4,128]{3,2,1,0:T(4,128)(2,1)}), bf16[16,9,4,128]{3,2,1,0:T(4,128)(2,1)S(1)}, u32[]{:S(2)}, u32[]{:S(2)}) %all-to-all-start) | async-done | bytes 147488 | tf_op jit(solution)/shard_map/all_to_all | solution.py:326
  31.1 0.5 shard_map.112
  31.6 0.0 copy-start.1
  31.6 1.4 %copy-done.1 = bf16[16,576,128]{2,1,0:T(8,128)(2,1)} copy-done((bf16[16,576,128]{2,1,0:T(8,128)(2,1)}, bf16[16,576,128]{2,1,0:T(8,128)(2,1)S(1)}, u32[]{:S(2)}) %copy-start.1) | copy-done | bytes 2359320
  33.0 8.9 %all-to-all-start.1 = ((bf16[16,576,128]{2,1,0:T(8,128)(2,1)}), bf16[16,576,128]{2,1,0:T(8,128)(2,1)S(1)}, u32[]{:S(2)}, u32[]{:S(2)}) async-start(bf16[16,576,128]{2,1,0:T(8,128)(2,1)} %copy-done.1), calls=%async_computation.1 | async-start | bytes 4718592 | tf_op jit(solution)/shard_map/all_to_all | solution.py:326
  42.0 0.0 copy-start.4
  42.0 0.0 copy-start.5
  42.0 3.5 %collective-permute-start = (bf16[6144,128]{1,0:T(8,128)(2,1)}, bf16[6144,128]{1,0:T(8,128)(2,1)S(1)}, u32[]{:S(2)}, u32[]{:S(2)}) collective-permute-start(bf16[6144,128]{1,0:T(8,128)(2,1)} %copy-done.15), channel_id=1, source_target_pairs={{0,16},{16,0},{1,17},{17,1},{2,18},{18,2},{3,19},{19,3},{4,20},{20... | collective-permute-start | bytes 4718600 | tf_op jit(solution)/shard_map/ppermute | solution.py:330
  45.4 3.2 %collective-permute-done.in_ref = bf16[6144,128]{1,0:T(8,128)(2,1)S(1)} collective-permute-done((bf16[6144,128]{1,0:T(8,128)(2,1)}, bf16[6144,128]{1,0:T(8,128)(2,1)S(1)}, u32[]{:S(2)}, u32[]{:S(2)}) %collective-permute-start) | collective-permute-done | bytes 1572896 | tf_op jit(solution)/shard_map/ppermute | solution.py:330
  48.7 0.0 copy-start.2
  48.7 1.1 copy-done.2
  49.8 21.3 %all-to-all-done.1.own_ref = bf16[16,576,128]{2,1,0:T(8,128)(2,1)S(1)} async-done(((bf16[16,576,128]{2,1,0:T(8,128)(2,1)}), bf16[16,576,128]{2,1,0:T(8,128)(2,1)S(1)}, u32[]{:S(2)}, u32[]{:S(2)}) %all-to-all-start.1) | async-done | bytes 2359328 | tf_op jit(solution)/shard_map/all_to_all | solution.py:326
  71.2 0.0 copy-done.4
  71.2 0.0 copy-done.5
  71.2 0.0 copy-start.3
  71.2 1.4 %copy-done.3 = bf16[6144,128]{1,0:T(8,128)(2,1)S(1)} copy-done((bf16[6144,128]{1,0:T(8,128)(2,1)S(1)}, bf16[6144,128]{1,0:T(8,128)(2,1)}, u32[]{:S(2)}) %copy-start.3) | copy-done | bytes 1572888
  72.6 0.0 copy-start.6
  72.6 1.0 copy-done.6
  73.6 0.0 copy-start
  73.6 3.2 %shard_map.114 = (bf16[16,296,128]{2,1,0:T(8,128)(2,1)}, bf16[288,512]{1,0:T(8,128)(2,1)S(1)}, bf16[288,256]{1,0:T(8,128)(2,1)S(1)}) custom-call(bf16[16,576,128]{2,1,0:T(8,128)(2,1)S(1)} %all-to-all-done.1.own_ref, bf16[2048,128]{1,0:T(8,128)(2,1)S(1)} %bitcast.14, bf16[2048,128]{1,0:T(8,128)(2,1)S(1)} %bitcast.16, bf16[128,2048]{1,0:T(8,128)(2,1)S(1)} %bitcast.18, ...), custom_call_target="tpu_custom_call" | custom-call | tf_op jit(solution)/shard_map/pallas_call | solution.py:371
  76.8 0.0 copy-done
  76.9 0.0 copy-start.7
  76.9 0.0 copy-start.9
  76.9 0.0 copy-start.16
  76.9 2.9 %shard_map.118 = bf16[384,2048]{1,0:T(8,128)(2,1)S(1)} custom-call(bf16[16,576,128]{2,1,0:T(8,128)(2,1)} %copy-done, bf16[288,512]{1,0:T(8,128)(2,1)S(1)} %get-tuple-element.24.both_ref, bf16[288,256]{1,0:T(8,128)(2,1)S(1)} %get-tuple-element.25.hidden_ref), custom_call_target="tpu_custom_call" | custom-call | tf_op jit(solution)/shard_map/pallas_call | solution.py:379
  79.8 0.0 copy-done.7
  79.8 0.0 copy-done.9
  79.8 3.5 %collective-permute-start.1 = (bf16[384,2048]{1,0:T(8,128)(2,1)S(1)}, bf16[384,2048]{1,0:T(8,128)(2,1)S(1)}, u32[]{:S(2)}, u32[]{:S(2)}) collective-permute-start(bf16[384,2048]{1,0:T(8,128)(2,1)S(1)} %shard_map.118), channel_id=1, source_target_pairs={{0,16},{16,0},{1,17},{17,1},{2,18},{18,2},{3,19},{19,3},{4,20},{20... | collective-permute-start | bytes 4718600 | tf_op jit(solution)/shard_map/ppermute | solution.py:330
  83.3 0.0 copy-done.16
  83.3 21.8 %all_to_all.20.in_ref = bf16[16,296,128]{2,1,0:T(8,128)(2,1)S(1)} all-to-all(bf16[16,296,128]{2,1,0:T(8,128)(2,1)S(1)} %copy-done.16), channel_id=1, replica_groups={{10,11,15,14,13,12,0,1,2,3,7,6,5,4,8,9},{26,27,31,30,29,28,16,17,18,19,..., dimensions={0} | all-to-all | bytes 2424832 | tf_op jit(solution)/shard_map/all_to_all | solution.py:326
  105.1 0.0 copy-start.8
  105.1 1.0 shard_map.115
  106.1 12.4 %all-to-all-start.3 = ((bf16[16,5,4,128]{3,2,1,0:T(4,128)(2,1)}), bf16[16,5,4,128]{3,2,1,0:T(4,128)(2,1)S(1)}, u32[]{:S(2)}, u32[]{:S(2)}) async-start(bf16[16,5,4,128]{3,2,1,0:T(4,128)(2,1)} %bitcast.7), calls=%async_computation.3 | async-start | bytes 163840 | tf_op jit(solution)/shard_map/all_to_all | solution.py:326
  118.5 1.2 shard_map.116
  119.7 0.0 copy-start.11
  119.7 0.7 copy-done.11
  120.4 0.0 copy-start.13
  120.4 0.6 copy-done.13
  121.1 2.0 %all-to-all-done.3 = bf16[16,5,4,128]{3,2,1,0:T(4,128)(2,1)S(1)} async-done(((bf16[16,5,4,128]{3,2,1,0:T(4,128)(2,1)}), bf16[16,5,4,128]{3,2,1,0:T(4,128)(2,1)S(1)}, u32[]{:S(2)}, u32[]{:S(2)}) %all-to-all-start.3) | async-done | bytes 81952 | tf_op jit(solution)/shard_map/all_to_all | solution.py:326
  123.0 0.0 copy-start.12
  123.0 1.0 copy-done.12
  124.0 0.0 copy-start.14
  124.0 0.9 copy-done.14
  124.9 1.0 shard_map.117
  125.9 0.0 collective-permute-done.1.other_ref
  126.0 0.0 copy-done.8
  126.0 0.0 copy-start.10
  126.0 0.9 copy-done.10
  126.9 3.9 %shard_map.119 = (bf16[2048,128]{1,0:T(8,128)(2,1)}, bf16[2048,128]{1,0:T(8,128)(2,1)}, bf16[128,2048]{1,0:T(8,128)(2,1)}) custom-call(bf16[16,576,128]{2,1,0:T(8,128)(2,1)} %copy-done, bf16[288,512]{1,0:T(8,128)(2,1)S(1)} %copy-done.8, bf16[288,256]{1,0:T(8,128)(2,1)S(1)} %copy-done.10, bf16[384,2048]{1,0:T(8,128)(2,1)S(1)} %collective-permute-done.1.other_ref), custom_call_target="tpu_custom_call" | custom-call | tf_op jit(solution)/shard_map/pallas_call | solution.py:381
  (1 shorter events, 0.0 us)
Async XLA Ops:
  3.5 1.2 copy-start.15
  4.7 26.4 %all-to-all-start = ((bf16[16,9,4,128]{3,2,1,0:T(4,128)(2,1)}), bf16[16,9,4,128]{3,2,1,0:T(4,128)(2,1)S(1)}, u32[]{:S(2)}, u32[]{:S(2)}) async-start(bf16[16,9,4,128]{3,2,1,0:T(4,128)(2,1)} %bitcast.5), calls=%async_computation | async-start | bytes 294912 | tf_op jit(solution)/shard_map/all_to_all | solution.py:326
  31.6 1.4 %copy-start.1 = (bf16[16,576,128]{2,1,0:T(8,128)(2,1)}, bf16[16,576,128]{2,1,0:T(8,128)(2,1)S(1)}, u32[]{:S(2)}) copy-start(bf16[16,576,128]{2,1,0:T(8,128)(2,1)S(1)} %shard_map.112) | copy-start | bytes 7077892
  33.0 38.1 %all-to-all-start.1 = ((bf16[16,576,128]{2,1,0:T(8,128)(2,1)}), bf16[16,576,128]{2,1,0:T(8,128)(2,1)S(1)}, u32[]{:S(2)}, u32[]{:S(2)}) async-start(bf16[16,576,128]{2,1,0:T(8,128)(2,1)} %copy-done.1), calls=%async_computation.1 | async-start | bytes 4718592 | tf_op jit(solution)/shard_map/all_to_all | solution.py:326
  42.0 29.2 %copy-start.4 = (bf16[1,2048,128]{2,1,0:T(8,128)(2,1)S(1)}, bf16[1,2048,128]{2,1,0:T(8,128)(2,1)}, u32[]{:S(2)}) copy-start(bf16[1,2048,128]{2,1,0:T(8,128)(2,1)} %param.11) | copy-start | bytes 1572868
  42.0 29.2 %copy-start.5 = (bf16[1,2048,128]{2,1,0:T(8,128)(2,1)S(1)}, bf16[1,2048,128]{2,1,0:T(8,128)(2,1)}, u32[]{:S(2)}) copy-start(bf16[1,2048,128]{2,1,0:T(8,128)(2,1)} %param.12) | copy-start | bytes 1572868
  42.0 6.7 %collective-permute-start = (bf16[6144,128]{1,0:T(8,128)(2,1)}, bf16[6144,128]{1,0:T(8,128)(2,1)S(1)}, u32[]{:S(2)}, u32[]{:S(2)}) collective-permute-start(bf16[6144,128]{1,0:T(8,128)(2,1)} %copy-done.15), channel_id=1, source_target_pairs={{0,16},{16,0},{1,17},{17,1},{2,18},{18,2},{3,19},{19,3},{4,20},{20... | collective-permute-start | bytes 4718600 | tf_op jit(solution)/shard_map/ppermute | solution.py:330
  48.7 1.2 copy-start.2
  71.2 1.4 %copy-start.3 = (bf16[6144,128]{1,0:T(8,128)(2,1)S(1)}, bf16[6144,128]{1,0:T(8,128)(2,1)}, u32[]{:S(2)}) copy-start(bf16[6144,128]{1,0:T(8,128)(2,1)} %shard_map.113.swap_ref) | copy-start | bytes 4718596
  72.6 1.0 copy-start.6
  73.6 3.2 %copy-start = (bf16[16,576,128]{2,1,0:T(8,128)(2,1)}, bf16[16,576,128]{2,1,0:T(8,128)(2,1)S(1)}, u32[]{:S(2)}) copy-start(bf16[16,576,128]{2,1,0:T(8,128)(2,1)S(1)} %all-to-all-done.1.own_ref) | copy-start | bytes 7077892
  76.9 2.9 %copy-start.7 = (bf16[288,512]{1,0:T(8,128)(2,1)}, bf16[288,512]{1,0:T(8,128)(2,1)S(1)}, u32[]{:S(2)}) copy-start(bf16[288,512]{1,0:T(8,128)(2,1)S(1)} %get-tuple-element.24.both_ref) | copy-start | bytes 884740
  76.9 2.9 %copy-start.9 = (bf16[288,256]{1,0:T(8,128)(2,1)}, bf16[288,256]{1,0:T(8,128)(2,1)S(1)}, u32[]{:S(2)}) copy-start(bf16[288,256]{1,0:T(8,128)(2,1)S(1)} %get-tuple-element.25.hidden_ref) | copy-start | bytes 442372
  76.9 6.4 %copy-start.16 = (bf16[16,296,128]{2,1,0:T(8,128)(2,1)S(1)}, bf16[16,296,128]{2,1,0:T(8,128)(2,1)}, u32[]{:S(2)}) copy-start(bf16[16,296,128]{2,1,0:T(8,128)(2,1)} %get-tuple-element.19) | copy-start | bytes 3637252
  79.8 46.2 %collective-permute-start.1 = (bf16[384,2048]{1,0:T(8,128)(2,1)S(1)}, bf16[384,2048]{1,0:T(8,128)(2,1)S(1)}, u32[]{:S(2)}, u32[]{:S(2)}) collective-permute-start(bf16[384,2048]{1,0:T(8,128)(2,1)S(1)} %shard_map.118), channel_id=1, source_target_pairs={{0,16},{16,0},{1,17},{17,1},{2,18},{18,2},{3,19},{19,3},{4,20},{20... | collective-permute-start | bytes 4718600 | tf_op jit(solution)/shard_map/ppermute | solution.py:330
  105.1 20.9 %copy-start.8 = (bf16[288,512]{1,0:T(8,128)(2,1)S(1)}, bf16[288,512]{1,0:T(8,128)(2,1)}, u32[]{:S(2)}) copy-start(bf16[288,512]{1,0:T(8,128)(2,1)} %copy-done.7) | copy-start | bytes 884740
  106.1 16.9 %all-to-all-start.3 = ((bf16[16,5,4,128]{3,2,1,0:T(4,128)(2,1)}), bf16[16,5,4,128]{3,2,1,0:T(4,128)(2,1)S(1)}, u32[]{:S(2)}, u32[]{:S(2)}) async-start(bf16[16,5,4,128]{3,2,1,0:T(4,128)(2,1)} %bitcast.7), calls=%async_computation.3 | async-start | bytes 163840 | tf_op jit(solution)/shard_map/all_to_all | solution.py:326
  119.7 0.7 copy-start.11
  120.4 0.6 copy-start.13
  123.0 1.0 copy-start.12
  124.0 0.9 copy-start.14
  126.0 0.9 copy-start.10
where the time goes:
time: 131 us
  starting transfers between devices  47.4 us (36%)
  waiting for transfers between devices  33.6 us (26%)
  blocking collectives  21.8 us (17%)
  Pallas kernels  16.8 us (13%)
  local copies, waits for them, and re-layouts  10.3 us (8%)
    all_to_all x3, starting transfers between devices, exchange(): lax.all_to_all(value, axis, 0, 0, axis_index_groups=groups, tiled=True)  40.4 us
    all_to_all x3, waiting for transfers between devices, exchange(): lax.all_to_all(value, axis, 0, 0, axis_index_groups=groups, tiled=True)  30.4 us
    all_to_all x1, blocking collectives, exchange(): lax.all_to_all(value, axis, 0, 0, axis_index_groups=groups, tiled=True)  21.8 us
    unnamed x34, local copies, waits for them, and re-layouts  10.3 us
    ppermute x2, starting transfers between devices, to_partner(): return lax.ppermute(value, 'ep_1', [(0, 1), (1, 0)])  6.99 us
    pallas_call x1, Pallas kernels, steps(): kernel(own_grads_kernel, out_shape=(shape((width, 128)), shape((width, 12...  3.86 us
    ppermute x2, waiting for transfers between devices, to_partner(): return lax.ppermute(value, 'ep_1', [(0, 1), (1, 0)])  3.23 us
    pallas_call x1, Pallas kernels, steps(): kernel(main_kernel, in_specs=[vmem] * 5, out_specs=(hbm, vmem, vmem), out...  3.22 us
  transfers between devices with their start and end apart: 5, of which 4 were waited for; matrix products, arithmetic and copies ran while one was open for 0% of the time, Pallas kernels for 3%

commit v1 on v0

--- a/solution.py
+++ b/solution.py
@@ -46,12 +46,12 @@
 
 
 def member_at(place):
-    return (place + 8) & 15
+    return (place + 10) & 15
 
 
 def own_lanes():
     z = lax.axis_index("ep_0")
-    place = (z + 8) % 16
+    place = (z + 6) % 16
     return (place % 4) * 32
 
 
@@ -322,7 +322,7 @@
 
 
 def exchange(value, axis):
-    groups = [[(k + 8) % 16 for k in range(16)]] if axis == "ep_0" else [list(TP_ORDER)]
+    groups = [[(k + 10) % 16 for k in range(16)]] if axis == "ep_0" else [list(TP_ORDER)]
     return lax.all_to_all(value, axis, 0, 0, axis_index_groups=groups, tiled=True)
 
 

time: 131 us -> 131 us (level)
    all_to_all x3, starting transfers between devices: 40.4 us -> 38.5 us  [exchange(): lax.all_to_all(value, axis, 0, 0, axis_index_groups=groups, tiled=True)]
where the time goes in v1:
time: 131 us; the launch traced here: 130 us
  starting transfers between devices  46.2 us (35%)
  waiting for transfers between devices  34 us (26%)
  blocking collectives  21.8 us (17%)
  Pallas kernels  16.8 us (13%)
  local copies, waits for them, and re-layouts  10.3 us (8%)
    all_to_all x3, starting transfers between devices, exchange(): lax.all_to_all(value, axis, 0, 0, axis_index_groups=groups, tiled=True)  38.5 us
    all_to_all x3, waiting for transfers between devices, exchange(): lax.all_to_all(value, axis, 0, 0, axis_index_groups=groups, tiled=True)  30.8 us
    all_to_all x1, blocking collectives, exchange(): lax.all_to_all(value, axis, 0, 0, axis_index_groups=groups, tiled=True)  21.8 us
    unnamed x34, local copies, waits for them, and re-layouts  10.3 us
    ppermute x2, starting transfers between devices, to_partner(): return lax.ppermute(value, 'ep_1', [(0, 1), (1, 0)])  7.71 us
    pallas_call x1, Pallas kernels, steps(): kernel(own_grads_kernel, out_shape=(shape((width, 128)), shape((width, 12...  3.86 us
    ppermute x2, waiting for transfers between devices, to_partner(): return lax.ppermute(value, 'ep_1', [(0, 1), (1, 0)])  3.23 us
    pallas_call x1, Pallas kernels, steps(): kernel(main_kernel, in_specs=[vmem] * 5, out_specs=(hbm, vmem, vmem), out...  3.22 us
  transfers between devices with their start and end apart: 5, of which 4 were waited for; matrix products, arithmetic and copies ran while one was open for 0% of the time, Pallas kernels for 3%

profile of v1, /device:TPU:1, one launch (start us, length us, event | category | flops | bytes accessed | tf_op | source)
XLA Modules:
  0.0 129.9 jit_solution(3518188296660345286)
XLA Ops:
  0.6 2.9 %shard_map.110 = (bf16[576,128]{1,0:T(8,128)(2,1)}, bf16[6144,128]{1,0:T(8,128)(2,1)S(1)}) custom-call(s32[2,128]{1,0:T(2,128)} %bitcast.21, f32[2,128]{1,0:T(2,128)} %bitcast.23, bf16[128,2048]{1,0:T(8,128)(2,1)} %tokens_ref.1, bf16[128,2048]{1,0:T(8,128)(2,1)} %grad_ref.1, bf16[2048,128]{1,0:T(8,128)(2,1)} %bitcast.13, bf16[2048,128]{1,0:T(8,128)(2,1)} %bitcast.15, ...), custom_call_target="tpu_custom_call" | custom-call | tf_op jit(solution)/shard_map/pallas_call | solution.py:344
  3.5 0.0 copy-start.15
  3.5 1.1 copy-done.15
  4.7 17.3 %all-to-all-start = ((bf16[16,9,4,128]{3,2,1,0:T(4,128)(2,1)}), bf16[16,9,4,128]{3,2,1,0:T(4,128)(2,1)S(1)}, u32[]{:S(2)}, u32[]{:S(2)}) async-start(bf16[16,9,4,128]{3,2,1,0:T(4,128)(2,1)} %bitcast.5), calls=%async_computation | async-start | bytes 294912 | tf_op jit(solution)/shard_map/all_to_all | solution.py:326
  22.0 0.2 shard_map.111.pick_ref
  22.2 8.1 %all-to-all-done = bf16[16,9,4,128]{3,2,1,0:T(4,128)(2,1)S(1)} async-done(((bf16[16,9,4,128]{3,2,1,0:T(4,128)(2,1)}), bf16[16,9,4,128]{3,2,1,0:T(4,128)(2,1)S(1)}, u32[]{:S(2)}, u32[]{:S(2)}) %all-to-all-start) | async-done | bytes 147488 | tf_op jit(solution)/shard_map/all_to_all | solution.py:326
  30.3 0.5 shard_map.112
  30.8 0.0 copy-start.1
  30.9 1.4 %copy-done.1 = bf16[16,576,128]{2,1,0:T(8,128)(2,1)} copy-done((bf16[16,576,128]{2,1,0:T(8,128)(2,1)}, bf16[16,576,128]{2,1,0:T(8,128)(2,1)S(1)}, u32[]{:S(2)}) %copy-start.1) | copy-done | bytes 2359320
  32.3 8.9 %all-to-all-start.1 = ((bf16[16,576,128]{2,1,0:T(8,128)(2,1)}), bf16[16,576,128]{2,1,0:T(8,128)(2,1)S(1)}, u32[]{:S(2)}, u32[]{:S(2)}) async-start(bf16[16,576,128]{2,1,0:T(8,128)(2,1)} %copy-done.1), calls=%async_computation.1 | async-start | bytes 4718592 | tf_op jit(solution)/shard_map/all_to_all | solution.py:326
  41.2 0.0 copy-start.4
  41.2 0.0 copy-start.5
  41.2 3.9 %collective-permute-start = (bf16[6144,128]{1,0:T(8,128)(2,1)}, bf16[6144,128]{1,0:T(8,128)(2,1)S(1)}, u32[]{:S(2)}, u32[]{:S(2)}) collective-permute-start(bf16[6144,128]{1,0:T(8,128)(2,1)} %copy-done.15), channel_id=1, source_target_pairs={{0,16},{16,0},{1,17},{17,1},{2,18},{18,2},{3,19},{19,3},{4,20},{20... | collective-permute-start | bytes 4718600 | tf_op jit(solution)/shard_map/ppermute | solution.py:330
  45.2 3.2 %collective-permute-done.in_ref = bf16[6144,128]{1,0:T(8,128)(2,1)S(1)} collective-permute-done((bf16[6144,128]{1,0:T(8,128)(2,1)}, bf16[6144,128]{1,0:T(8,128)(2,1)S(1)}, u32[]{:S(2)}, u32[]{:S(2)}) %collective-permute-start) | collective-permute-done | bytes 1572896 | tf_op jit(solution)/shard_map/ppermute | solution.py:330
  48.4 0.0 copy-start.2
  48.4 1.1 copy-done.2
  49.5 19.2 %all-to-all-done.1.own_ref = bf16[16,576,128]{2,1,0:T(8,128)(2,1)S(1)} async-done(((bf16[16,576,128]{2,1,0:T(8,128)(2,1)}), bf16[16,576,128]{2,1,0:T(8,128)(2,1)S(1)}, u32[]{:S(2)}, u32[]{:S(2)}) %all-to-all-start.1) | async-done | bytes 2359328 | tf_op jit(solution)/shard_map/all_to_all | solution.py:326
  68.8 0.0 copy-done.4
  68.8 0.0 copy-done.5
  68.8 0.0 copy-start.3
  68.8 1.4 %copy-done.3 = bf16[6144,128]{1,0:T(8,128)(2,1)S(1)} copy-done((bf16[6144,128]{1,0:T(8,128)(2,1)S(1)}, bf16[6144,128]{1,0:T(8,128)(2,1)}, u32[]{:S(2)}) %copy-start.3) | copy-done | bytes 1572888
  70.2 0.0 copy-start.6
  70.2 1.0 copy-done.6
  71.2 0.0 copy-start
  71.2 3.2 %shard_map.114 = (bf16[16,296,128]{2,1,0:T(8,128)(2,1)}, bf16[288,512]{1,0:T(8,128)(2,1)S(1)}, bf16[288,256]{1,0:T(8,128)(2,1)S(1)}) custom-call(bf16[16,576,128]{2,1,0:T(8,128)(2,1)S(1)} %all-to-all-done.1.own_ref, bf16[2048,128]{1,0:T(8,128)(2,1)S(1)} %bitcast.14, bf16[2048,128]{1,0:T(8,128)(2,1)S(1)} %bitcast.16, bf16[128,2048]{1,0:T(8,128)(2,1)S(1)} %bitcast.18, ...), custom_call_target="tpu_custom_call" | custom-call | tf_op jit(solution)/shard_map/pallas_call | solution.py:371
  74.5 0.0 copy-done
  74.5 0.0 copy-start.7
  74.5 0.0 copy-start.9
  74.5 0.0 copy-start.16
  74.5 2.9 %shard_map.118 = bf16[384,2048]{1,0:T(8,128)(2,1)S(1)} custom-call(bf16[16,576,128]{2,1,0:T(8,128)(2,1)} %copy-done, bf16[288,512]{1,0:T(8,128)(2,1)S(1)} %get-tuple-element.24.both_ref, bf16[288,256]{1,0:T(8,128)(2,1)S(1)} %get-tuple-element.25.hidden_ref), custom_call_target="tpu_custom_call" | custom-call | tf_op jit(solution)/shard_map/pallas_call | solution.py:379
  77.4 0.0 copy-done.7
  77.4 0.0 copy-done.9
  77.4 3.8 %collective-permute-start.1 = (bf16[384,2048]{1,0:T(8,128)(2,1)S(1)}, bf16[384,2048]{1,0:T(8,128)(2,1)S(1)}, u32[]{:S(2)}, u32[]{:S(2)}) collective-permute-start(bf16[384,2048]{1,0:T(8,128)(2,1)S(1)} %shard_map.118), channel_id=1, source_target_pairs={{0,16},{16,0},{1,17},{17,1},{2,18},{18,2},{3,19},{19,3},{4,20},{20... | collective-permute-start | bytes 4718600 | tf_op jit(solution)/shard_map/ppermute | solution.py:330
  81.2 0.0 copy-done.16
  81.2 21.8 %all_to_all.20.in_ref = bf16[16,296,128]{2,1,0:T(8,128)(2,1)S(1)} all-to-all(bf16[16,296,128]{2,1,0:T(8,128)(2,1)S(1)} %copy-done.16), channel_id=1, replica_groups={{10,11,15,14,13,12,0,1,2,3,7,6,5,4,8,9},{26,27,31,30,29,28,16,17,18,19,..., dimensions={0} | all-to-all | bytes 2424832 | tf_op jit(solution)/shard_map/all_to_all | solution.py:326
  103.0 0.0 copy-start.8
  103.0 1.0 shard_map.115
  104.0 12.3 %all-to-all-start.3 = ((bf16[16,5,4,128]{3,2,1,0:T(4,128)(2,1)}), bf16[16,5,4,128]{3,2,1,0:T(4,128)(2,1)S(1)}, u32[]{:S(2)}, u32[]{:S(2)}) async-start(bf16[16,5,4,128]{3,2,1,0:T(4,128)(2,1)} %bitcast.7), calls=%async_computation.3 | async-start | bytes 163840 | tf_op jit(solution)/shard_map/all_to_all | solution.py:326
  116.3 1.2 shard_map.116
  117.5 0.0 copy-start.11
  117.5 0.7 copy-done.11
  118.2 0.0 copy-start.13
  118.2 0.6 copy-done.13
  118.8 3.4 %all-to-all-done.3 = bf16[16,5,4,128]{3,2,1,0:T(4,128)(2,1)S(1)} async-done(((bf16[16,5,4,128]{3,2,1,0:T(4,128)(2,1)}), bf16[16,5,4,128]{3,2,1,0:T(4,128)(2,1)S(1)}, u32[]{:S(2)}, u32[]{:S(2)}) %all-to-all-start.3) | async-done | bytes 81952 | tf_op jit(solution)/shard_map/all_to_all | solution.py:326
  122.3 0.0 copy-start.12
  122.3 1.0 copy-done.12
  123.2 0.0 copy-start.14
  123.2 0.9 copy-done.14
  124.1 1.0 shard_map.117
  125.2 0.0 collective-permute-done.1.other_ref
  125.2 0.0 copy-done.8
  125.2 0.0 copy-start.10
  125.2 0.9 copy-done.10
  126.1 3.9 %shard_map.119 = (bf16[2048,128]{1,0:T(8,128)(2,1)}, bf16[2048,128]{1,0:T(8,128)(2,1)}, bf16[128,2048]{1,0:T(8,128)(2,1)}) custom-call(bf16[16,576,128]{2,1,0:T(8,128)(2,1)} %copy-done, bf16[288,512]{1,0:T(8,128)(2,1)S(1)} %copy-done.8, bf16[288,256]{1,0:T(8,128)(2,1)S(1)} %copy-done.10, bf16[384,2048]{1,0:T(8,128)(2,1)S(1)} %collective-permute-done.1.other_ref), custom_call_target="tpu_custom_call" | custom-call | tf_op jit(solution)/shard_map/pallas_call | solution.py:381
  (1 shorter events, 0.0 us)
Async XLA Ops:
  3.5 1.2 copy-start.15
  4.7 25.7 %all-to-all-start = ((bf16[16,9,4,128]{3,2,1,0:T(4,128)(2,1)}), bf16[16,9,4,128]{3,2,1,0:T(4,128)(2,1)S(1)}, u32[]{:S(2)}, u32[]{:S(2)}) async-start(bf16[16,9,4,128]{3,2,1,0:T(4,128)(2,1)} %bitcast.5), calls=%async_computation | async-start | bytes 294912 | tf_op jit(solution)/shard_map/all_to_all | solution.py:326
  30.8 1.4 %copy-start.1 = (bf16[16,576,128]{2,1,0:T(8,128)(2,1)}, bf16[16,576,128]{2,1,0:T(8,128)(2,1)S(1)}, u32[]{:S(2)}) copy-start(bf16[16,576,128]{2,1,0:T(8,128)(2,1)S(1)} %shard_map.112) | copy-start | bytes 7077892
  32.3 36.5 %all-to-all-start.1 = ((bf16[16,576,128]{2,1,0:T(8,128)(2,1)}), bf16[16,576,128]{2,1,0:T(8,128)(2,1)S(1)}, u32[]{:S(2)}, u32[]{:S(2)}) async-start(bf16[16,576,128]{2,1,0:T(8,128)(2,1)} %copy-done.1), calls=%async_computation.1 | async-start | bytes 4718592 | tf_op jit(solution)/shard_map/all_to_all | solution.py:326
  41.2 27.6 %copy-start.4 = (bf16[1,2048,128]{2,1,0:T(8,128)(2,1)S(1)}, bf16[1,2048,128]{2,1,0:T(8,128)(2,1)}, u32[]{:S(2)}) copy-start(bf16[1,2048,128]{2,1,0:T(8,128)(2,1)} %param.11) | copy-start | bytes 1572868
  41.2 27.6 %copy-start.5 = (bf16[1,2048,128]{2,1,0:T(8,128)(2,1)S(1)}, bf16[1,2048,128]{2,1,0:T(8,128)(2,1)}, u32[]{:S(2)}) copy-start(bf16[1,2048,128]{2,1,0:T(8,128)(2,1)} %param.12) | copy-start | bytes 1572868
  41.2 7.2 %collective-permute-start = (bf16[6144,128]{1,0:T(8,128)(2,1)}, bf16[6144,128]{1,0:T(8,128)(2,1)S(1)}, u32[]{:S(2)}, u32[]{:S(2)}) collective-permute-start(bf16[6144,128]{1,0:T(8,128)(2,1)} %copy-done.15), channel_id=1, source_target_pairs={{0,16},{16,0},{1,17},{17,1},{2,18},{18,2},{3,19},{19,3},{4,20},{20... | collective-permute-start | bytes 4718600 | tf_op jit(solution)/shard_map/ppermute | solution.py:330
  48.4 1.2 copy-start.2
  68.8 1.4 %copy-start.3 = (bf16[6144,128]{1,0:T(8,128)(2,1)S(1)}, bf16[6144,128]{1,0:T(8,128)(2,1)}, u32[]{:S(2)}) copy-start(bf16[6144,128]{1,0:T(8,128)(2,1)} %shard_map.113.swap_ref) | copy-start | bytes 4718596
  70.2 1.0 copy-start.6
  71.2 3.2 %copy-start = (bf16[16,576,128]{2,1,0:T(8,128)(2,1)}, bf16[16,576,128]{2,1,0:T(8,128)(2,1)S(1)}, u32[]{:S(2)}) copy-start(bf16[16,576,128]{2,1,0:T(8,128)(2,1)S(1)} %all-to-all-done.1.own_ref) | copy-start | bytes 7077892
  74.5 2.9 %copy-start.7 = (bf16[288,512]{1,0:T(8,128)(2,1)}, bf16[288,512]{1,0:T(8,128)(2,1)S(1)}, u32[]{:S(2)}) copy-start(bf16[288,512]{1,0:T(8,128)(2,1)S(1)} %get-tuple-element.24.both_ref) | copy-start | bytes 884740
  74.5 2.9 %copy-start.9 = (bf16[288,256]{1,0:T(8,128)(2,1)}, bf16[288,256]{1,0:T(8,128)(2,1)S(1)}, u32[]{:S(2)}) copy-start(bf16[288,256]{1,0:T(8,128)(2,1)S(1)} %get-tuple-element.25.hidden_ref) | copy-start | bytes 442372
  74.5 6.7 %copy-start.16 = (bf16[16,296,128]{2,1,0:T(8,128)(2,1)S(1)}, bf16[16,296,128]{2,1,0:T(8,128)(2,1)}, u32[]{:S(2)}) copy-start(bf16[16,296,128]{2,1,0:T(8,128)(2,1)} %get-tuple-element.19) | copy-start | bytes 3637252
  77.4 47.8 %collective-permute-start.1 = (bf16[384,2048]{1,0:T(8,128)(2,1)S(1)}, bf16[384,2048]{1,0:T(8,128)(2,1)S(1)}, u32[]{:S(2)}, u32[]{:S(2)}) collective-permute-start(bf16[384,2048]{1,0:T(8,128)(2,1)S(1)} %shard_map.118), channel_id=1, source_target_pairs={{0,16},{16,0},{1,17},{17,1},{2,18},{18,2},{3,19},{19,3},{4,20},{20... | collective-permute-start | bytes 4718600 | tf_op jit(solution)/shard_map/ppermute | solution.py:330
  103.0 22.2 %copy-start.8 = (bf16[288,512]{1,0:T(8,128)(2,1)S(1)}, bf16[288,512]{1,0:T(8,128)(2,1)}, u32[]{:S(2)}) copy-start(bf16[288,512]{1,0:T(8,128)(2,1)} %copy-done.7) | copy-start | bytes 884740
  104.0 18.3 %all-to-all-start.3 = ((bf16[16,5,4,128]{3,2,1,0:T(4,128)(2,1)}), bf16[16,5,4,128]{3,2,1,0:T(4,128)(2,1)S(1)}, u32[]{:S(2)}, u32[]{:S(2)}) async-start(bf16[16,5,4,128]{3,2,1,0:T(4,128)(2,1)} %bitcast.7), calls=%async_computation.3 | async-start | bytes 163840 | tf_op jit(solution)/shard_map/all_to_all | solution.py:326
  117.5 0.7 copy-start.11
  118.2 0.6 copy-start.13
  122.3 1.0 copy-start.12
  123.2 0.9 copy-start.14
  125.2 0.9 copy-start.10
